TPU v7x, 512 devices: a whole 4x8x8 slice. The times are simulated.
512 devices in a mesh: sp: 32 (over z, x), tp: 16 (over y, core).
Axes of the slice: x: 4, y: 8, z: 8, core: 2. Of those that a mesh axis runs over, the one named last changes fastest.
Arguments:
- lane_source_signal: bfloat16 [1024, 4096], P('tp', 'sp'), may hold values from -6 to 6
- spectral_damping_part: float32 [64, 64], P('tp'), may hold values from -3 to -0.0002
- spectral_angular_part: float32 [64, 64], P('tp'), may hold values from 0.31 to 201.0624
- interval_exponent: float32 [64], P('tp'), may hold values from -3.9 to -1.6
- entry_matrix_inphase: float32 [64, 64, 16], P('tp'), may hold values from -1 to 1
- entry_matrix_quadrature: float32 [64, 64, 16], P('tp'), may hold values from -1 to 1
- emission_inphase: float32 [64, 16, 64], P('tp'), may hold values from -0.75 to 0.75
- emission_quadrature: float32 [64, 16, 64], P('tp'), may hold values from -0.75 to 0.75
- lane_bypass_factor: float32 [1024], P('tp'), may hold values from -5 to 5
- spike_shrink_offset: float32 [64, 4096], P('tp', 'sp'), may hold values from -1.4 to 0
- lane_exit_matrix: bfloat16 [1024, 4096], P('tp'), may hold values from -0.1875 to 0.1875
- skipline_stream: bfloat16 [4096, 4096], P('sp'), may hold values from -6 to 6
- specialist_scaling_vector: float32 [4096], replicated, may hold values from 0.1 to 1.9
- selected_specialists: int32 [4096, 2], P('sp'), may hold values from 0 to 31, all different within a row; in each aligned block of 128 rows (0 to 127, 128 to 255, ...) at most 16 rows name the same one
- dispatcher_scores: float32 [4096, 2], P('sp'), may hold values from 0.1 to 1
- specialist_valve_matrix: bfloat16 [32, 4096, 2048], P('sp', None, 'tp'), may hold values from -0.09375 to 0.09375
- specialist_widen_matrix: bfloat16 [32, 4096, 2048], P('sp', None, 'tp'), may hold values from -0.09375 to 0.09375
- specialist_shrink_matrix: bfloat16 [32, 2048, 4096], P('sp', 'tp'), may hold values from -0.1875 to 0.1875
Outputs:
- updated: bfloat16 [4096, 4096], P('sp', 'tp')
Inputs may be any that keep to these rules, and one draw needn't show every extreme that they name: `selected_specialists`: each row names 2 different experts. Among the rows of each aligned block of 128 positions no expert is named more than 16 times, and in every block some expert is named exactly 16 times.
All inputs are finite; a program needn't handle non-finite values.
Results may differ from a plain program's by a relative error of at most 0.019.
Values may be sent and summed in bfloat16 or wider, within the bound.
A program may use at most 64 MiB of HBM per device.

v0:
```python
import jax
import jax.numpy as jnp
from jax import lax
from jax.sharding import PartitionSpec as P

EPS = 1e-06
PRECISE_MODE = lax.Precision.HIGHEST


def copy_for_each(array, axis):
    copies = jnp.broadcast_to(array, (lax.axis_size(axis), *array.shape))
    return lax.all_to_all(copies, axis, split_axis=0, concat_axis=0, tiled=True)


def gathered_once(array, axis):
    leaves = jax.tree.leaves(array)
    order = sorted(range(len(leaves)), key=lambda k: -leaves[k].size)
    width = (1, *leaves[order[0]].shape)[-1]
    lines = [
        jnp.pad(leaves[k].reshape(-1), (0, -leaves[k].size % width)).reshape(-1, width)
        for k in order
    ]
    both, at, found = (copy_for_each(jnp.concatenate(lines), axis), 0, {})
    for k, line in zip(order, lines):
        share = both[:, at : at + len(line)].reshape(len(both), -1)
        found[k] = share[:, : leaves[k].size].reshape(-1, *leaves[k].shape)
        at += len(line)
    numbers = iter(range(len(leaves)))
    return jax.tree.map(lambda _: found[next(numbers)], array)


def combined_pairwise(pieces, combine):
    while len(jax.tree.leaves(pieces)[0]) > 1:
        pieces = jax.vmap(combine)(
            *(jax.tree.map(lambda part: part[side::2], pieces) for side in (0, 1))
        )
    return jax.tree.map(lambda part: part[0], pieces)


def prefix(array, axis, combine, identity):
    length, mine = (lax.axis_size(axis), lax.axis_index(axis))
    passed = jnp.arange(length) < mine

    def kept(part, zero, own):
        part = jnp.where(
            passed.reshape(-1, *(1 for _ in own.shape)), part, jnp.asarray(zero, own.dtype)
        )
        return part

    pieces = gathered_once(array, axis)
    return combined_pairwise(jax.tree.map(kept, pieces, identity, array), combine)


def in_blocks(array, dim, length):
    before, after = (array.shape[:dim], array.shape[dim + 1 :])
    return jnp.moveaxis(array.reshape(*before, length, -1, *after), dim, 0)


def sent_and_summed(array, axis, dim):
    length = lax.axis_size(axis)
    parts = lax.all_to_all(in_blocks(array, dim, length), axis, 0, 0, tiled=True)
    return jnp.sum(parts.astype(jnp.float32), axis=0)


def taken_together(array, axis):
    return copy_for_each(array, axis).sum(axis=0)


def affine_pair(earlier, latter):
    mul_re = earlier[0] * latter[0] - earlier[1] * latter[1]
    mul_im = earlier[0] * latter[1] + earlier[1] * latter[0]
    add_re = latter[0] * earlier[2] - latter[1] * earlier[3] + latter[2]
    add_im = latter[0] * earlier[3] + latter[1] * earlier[2] + latter[3]
    return (mul_re, mul_im, add_re, add_im)


def local_prefix(elements):
    length = elements[0].shape[2]
    fills = (1.0, 0.0, 0.0, 0.0)
    offset = 1
    while offset < length:
        earlier = tuple(
            (
                jnp.pad(
                    item[:, :, : length - offset],
                    ((0, 0), (0, 0), (offset, 0)),
                    constant_values=fill,
                )
                for item, fill in zip(elements, fills)
            )
        )
        elements = affine_pair(earlier, elements)
        offset = offset * 2
    return elements


def per_device(
    lane_source_signal,
    spectral_damping_part,
    spectral_angular_part,
    interval_exponent,
    entry_matrix_inphase,
    entry_matrix_quadrature,
    emission_inphase,
    emission_quadrature,
    lane_bypass_factor,
    spike_shrink_offset,
    lane_exit_matrix,
    skipline_stream,
    specialist_scaling_vector,
    selected_specialists,
    dispatcher_scores,
    specialist_valve_matrix,
    specialist_widen_matrix,
    specialist_shrink_matrix,
):
    f32 = jnp.float32
    bf16 = jnp.bfloat16
    groups_here = spectral_damping_part.shape[0]
    lanes_within_bundle = entry_matrix_inphase.shape[2]
    tok_local = lane_source_signal.shape[1]
    bundled_signal = lane_source_signal.astype(f32).reshape(
        groups_here, lanes_within_bundle, tok_local
    )
    step_size = jnp.exp(interval_exponent)[:, None]
    natural_pace_exponent = spectral_damping_part * step_size
    angle = spectral_angular_part * step_size
    num_re = jnp.expm1(natural_pace_exponent) * jnp.cos(angle) - 2.0 * jnp.sin(0.5 * angle) ** 2
    num_im = jnp.exp(natural_pace_exponent) * jnp.sin(angle)
    denom = (
        spectral_damping_part * spectral_damping_part
        + spectral_angular_part * spectral_angular_part
    )
    fac_re = (num_re * spectral_damping_part + num_im * spectral_angular_part) / denom
    fac_im = (num_im * spectral_damping_part - num_re * spectral_angular_part) / denom
    map_re = (
        fac_re[:, :, None] * entry_matrix_inphase - fac_im[:, :, None] * entry_matrix_quadrature
    )
    map_im = (
        fac_re[:, :, None] * entry_matrix_quadrature + fac_im[:, :, None] * entry_matrix_inphase
    )
    drive_re = jnp.einsum("gpc,gct->gpt", map_re, bundled_signal, precision=PRECISE_MODE)
    drive_im = jnp.einsum("gpc,gct->gpt", map_im, bundled_signal, precision=PRECISE_MODE)
    recurrence_modulus = jnp.exp(
        natural_pace_exponent[:, :, None] + spike_shrink_offset[:, None, :]
    )
    trans_re = recurrence_modulus * jnp.cos(angle)[:, :, None]
    trans_im = recurrence_modulus * jnp.sin(angle)[:, :, None]
    cum_re, cum_im, state_real, state_imaginary = local_prefix(
        (trans_re, trans_im, drive_re, drive_im)
    )
    summary = (cum_re[:, :, -1], cum_im[:, :, -1], state_real[:, :, -1], state_imaginary[:, :, -1])
    unit = jnp.ones_like(summary[0])
    blank = jnp.zeros_like(summary[0])
    carried = prefix(summary, "sp", affine_pair, (unit, blank, blank, blank))
    enter_re = carried[2][:, :, None]
    enter_im = carried[3][:, :, None]
    state_real = state_real + cum_re * enter_re - cum_im * enter_im
    state_imaginary = state_imaginary + cum_re * enter_im + cum_im * enter_re
    value = (
        jnp.einsum("nef,nfi->nei", emission_inphase, state_real, precision=PRECISE_MODE)
        - jnp.einsum("nef,nfi->nei", emission_quadrature, state_imaginary, precision=PRECISE_MODE)
        + lane_bypass_factor.reshape(groups_here, lanes_within_bundle)[:, :, None] * bundled_signal
    )
    recurrence_result = (
        jax.nn.gelu(value).astype(bf16).reshape(groups_here * lanes_within_bundle, tok_local)
    )
    width = specialist_scaling_vector.shape[0]
    d_local = width // lax.axis_size("tp")
    col_start = lax.axis_index("tp") * d_local
    partial_rows = jnp.einsum(
        "ct,cd->td", recurrence_result, lane_exit_matrix, preferred_element_type=f32
    )
    projected_own = sent_and_summed(partial_rows.astype(jnp.bfloat16), "tp", 1).astype(bf16)
    own_residual = lax.dynamic_slice_in_dim(skipline_stream, col_start, d_local, 1)
    stream_own = (
        own_residual.astype(f32) + lax.optimization_barrier(projected_own).astype(f32)
    ).astype(bf16)
    own_stream = lax.optimization_barrier(stream_own).astype(f32)
    square_total = taken_together(jnp.sum(own_stream * own_stream, axis=1), "tp")
    inv_rms = lax.rsqrt(square_total / width + EPS)[:, None]
    own_gain = lax.dynamic_slice_in_dim(specialist_scaling_vector, col_start, d_local, 0)
    own_cols = (own_stream * inv_rms * own_gain).astype(bf16)
    share = dispatcher_scores / jnp.sum(dispatcher_scores, axis=1, keepdims=True)
    experts = lax.axis_size("sp")
    top = selected_specialists.shape[1]
    capacity = 2 * tok_local * top // experts
    flat_routes = selected_specialists.reshape(-1)
    hits = (flat_routes[:, None] == jnp.arange(experts, dtype=jnp.int32)[None, :]).astype(jnp.int32)
    ranks = jnp.sum((jnp.cumsum(hits, axis=0) - hits) * hits, axis=1)
    slot_ids = flat_routes * capacity + ranks
    slot_grid = jnp.arange(experts * capacity, dtype=jnp.int32)
    matched = slot_grid[:, None] == slot_ids[None, :]
    token_of = jnp.arange(tok_local * top, dtype=jnp.int32) // top
    slot_token = jnp.sum(jnp.where(matched, token_of[None, :], 0), axis=1)
    slot_live = jnp.any(matched, axis=1)
    gate_w = specialist_valve_matrix[0]
    up_w = specialist_widen_matrix[0]
    down_w = specialist_shrink_matrix[0]
    bf_zero = jnp.zeros((), bf16)
    dispatch = jnp.where(slot_live[:, None], own_cols[slot_token], bf_zero).reshape(
        experts, capacity, d_local
    )
    arrived = lax.all_to_all(dispatch, "sp", split_axis=0, concat_axis=0, tiled=True)
    piece = lax.all_gather(arrived, "tp", axis=2, tiled=True)
    gate_part = jnp.einsum("snd,df->snf", piece, gate_w, preferred_element_type=f32)
    up_part = jnp.einsum("snd,df->snf", piece, up_w, preferred_element_type=f32)
    hidden = (jax.nn.silu(gate_part) * up_part).astype(bf16)
    flat_hidden = hidden.reshape(experts * capacity, hidden.shape[2])
    down_part = jnp.dot(flat_hidden, down_w, preferred_element_type=f32).astype(bf16)
    summed = lax.psum_scatter(
        down_part.astype(f32).astype(jnp.bfloat16), "tp", scatter_dimension=1, tiled=True
    ).astype(jnp.float32)
    expert_out = summed.astype(bf16).reshape(experts, capacity, d_local)
    returned = lax.all_to_all(expert_out, "sp", split_axis=0, concat_axis=0, tiled=True).reshape(
        experts * capacity, d_local
    )
    picked = returned[slot_ids].reshape(tok_local, top, d_local)
    combined = jnp.sum(lax.optimization_barrier(picked).astype(f32) * share[:, :, None], axis=1)
    return (own_stream + combined).astype(bf16)


def solution(mesh):
    placed = (
        P("tp", "sp"),
        P("tp", None),
        P("tp", None),
        P("tp"),
        P("tp", None, None),
        P("tp", None, None),
        P("tp", None, None),
        P("tp", None, None),
        P("tp"),
        P("tp", "sp"),
        P("tp", None),
        P("sp", None),
        P(),
        P("sp", None),
        P("sp", None),
        P("sp", None, "tp"),
        P("sp", None, "tp"),
        P("sp", "tp", None),
    )
    return jax.shard_map(
        per_device, mesh=mesh, in_specs=placed, out_specs=P("sp", "tp"), check_vma=False
    )
```

profile of v0, /device:TPU:25, one launch (start us, length us, event | category | flops | bytes accessed | tf_op | source)
XLA Modules:
  0.0 256.6 jit_solution(5773878891755166815)
XLA Ops:
  6.5 0.7 exp.13
  7.3 0.8 fusion.57
  8.1 1.1 fusion.42
  9.2 1.1 fusion.46
  10.3 0.9 subtract_add_fusion.6
  11.2 1.0 add_add_fusion.5
  14.8 0.8 reshape.198
  15.6 12.9 %all-to-all-start = ((f32[32,1,1024]{2,1,0:T(1,128)}), f32[32,1,1024]{2,1,0:T(1,128)S(1)}, u32[]{:S(2)}, u32[]{:S(2)}) async-start(f32[32,1,1024]{2,1,0:T(1,128)} %reshape.198), calls=%async_computation | async-start | bytes 262144 | tf_op jit(solution)/shard_map/all_to_all | solution.py:12
  28.6 9.2 %all-to-all-done = f32[32,1,1024]{2,1,0:T(1,128)S(1)} async-done(((f32[32,1,1024]{2,1,0:T(1,128)}), f32[32,1,1024]{2,1,0:T(1,128)S(1)}, u32[]{:S(2)}, u32[]{:S(2)}) %all-to-all-start) | async-done | bytes 131104 | tf_op jit(solution)/shard_map/all_to_all | solution.py:12
  37.9 0.5 broadcast.191
  38.4 0.9 reduce.12
  40.5 0.4 convolution_convert_fusion.1
  40.9 1.1 copy.117
  42.0 9.1 %all-to-all-start.1 = ((bf16[16,128,256]{2,1,0:T(8,128)(2,1)}), bf16[16,128,256]{2,1,0:T(8,128)(2,1)S(1)}, u32[]{:S(2)}, u32[]{:S(2)}) async-start(bf16[16,128,256]{2,1,0:T(8,128)(2,1)} %bitcast.68), calls=%async_computation.1 | async-start | bytes 2097152 | tf_op jit(solution)/shard_map/all_to_all | solution.py:61
  51.6 0.6 reduce-window.6
  52.9 24.5 %all-to-all-done.1 = bf16[16,128,256]{2,1,0:T(8,128)(2,1)S(1)} async-done(((bf16[16,128,256]{2,1,0:T(8,128)(2,1)}), bf16[16,128,256]{2,1,0:T(8,128)(2,1)S(1)}, u32[]{:S(2)}, u32[]{:S(2)}) %all-to-all-start.1) | async-done | bytes 1048608 | tf_op jit(solution)/shard_map/all_to_all | solution.py:61
  77.5 0.9 add_convert_fusion
  78.5 0.6 broadcast_in_dim.86
  79.1 5.2 %all-to-all-start.2 = ((f32[16,1,128]{2,1,0:T(1,128)}), f32[16,1,128]{2,1,0:T(1,128)S(1)}, u32[]{:S(2)}, u32[]{:S(2)}) async-start(f32[16,1,128]{2,1,0:T(1,128)} %broadcast_in_dim.86), calls=%async_computation.2 | async-start | bytes 16384 | tf_op jit(solution)/shard_map/all_to_all | solution.py:12
  84.4 0.8 dynamic_slice.7
  85.3 3.2 %all-to-all-done.2 = f32[16,1,128]{2,1,0:T(1,128)S(1)} async-done(((f32[16,1,128]{2,1,0:T(1,128)}), f32[16,1,128]{2,1,0:T(1,128)S(1)}, u32[]{:S(2)}, u32[]{:S(2)}) %all-to-all-start.2) | async-done | bytes 8224 | tf_op jit(solution)/shard_map/all_to_all | solution.py:12
  88.6 2.0 gather_fusion
  90.7 15.2 %all_to_all.26 = bf16[32,16,256]{2,1,0:T(8,128)(2,1)} all-to-all(bf16[32,16,256]{2,1,0:T(8,128)(2,1)S(1)} %broadcast_select_fusion), channel_id=1, replica_groups=mesh['sp'=32,'tp'=16] {'sp'}, dimensions={0} | all-to-all | bytes 524288 | tf_op jit(solution)/shard_map/all_to_all | solution.py:204
  106.0 45.2 %all-gather.2.cloned.1.call-done = bf16[32,16,4096]{2,1,0:T(8,128)(2,1)} async-done(((bf16[32,16,256]{2,1,0:T(8,128)(2,1)}), bf16[32,16,4096]{2,1,0:T(8,128)(2,1)}) %all-gather.2.cloned.1.call-update) | async-done | bytes 4194320 | tf_op jit(solution)/shard_map/all_gather | solution.py:205
  151.2 3.6 %fusion.5 = f32[32,16,128]{2,1,0:T(8,128)S(1)} fusion(bf16[32,16,4096]{2,1,0:T(8,128)(2,1)} %all-gather.2.cloned.1.call-done, bf16[1,4096,128]{2,1,0:T(8,128)(2,1)S(1)} %copy-done.2), kind=kOutput, calls=%fused_computation.12 | convolution fusion | flops 536870912 | bytes 5505024 | tf_op jit(solution)/shard_map/snd,df->snf/dot_general | solution.py:206
  154.8 2.5 fusion
  157.3 3.2 %convolution_convert_fusion = bf16[512,4096]{1,0:T(8,128)(2,1)} fusion(bf16[512,128]{1,0:T(8,128)(2,1)S(1)} %bitcast.140, bf16[1,128,4096]{2,1,0:T(8,128)(2,1)S(1)} %copy-done), kind=kOutput, calls=%fused_computation.2 | convolution fusion | flops 538968064 | bytes 5373952 | tf_op jit(solution)/shard_map/dot_general | solution.py:210
  160.8 65.8 %reduce-scatter.2.cloned.1.call-done = bf16[512,256]{1,0:T(8,128)(2,1)} async-done(((bf16[512,4096]{1,0:T(8,128)(2,1)}), bf16[512,256]{1,0:T(8,128)(2,1)}) %reduce-scatter.2.cloned.1.call-update) | async-done | bytes 262160 | tf_op jit(solution)/shard_map/reduce_scatter | solution.py:211
  226.6 9.7 %all-to-all-start.4 = ((bf16[32,16,256]{2,1,0:T(8,128)(2,1)}), bf16[32,16,256]{2,1,0:T(8,128)(2,1)S(1)}, u32[]{:S(2)}, u32[]{:S(2)}) async-start(bf16[32,16,256]{2,1,0:T(8,128)(2,1)} %bitcast.141), calls=%async_computation.5 | async-start | bytes 524288 | tf_op jit(solution)/shard_map/all_to_all | solution.py:215
  236.5 11.0 %all-to-all-done.4 = bf16[32,16,256]{2,1,0:T(8,128)(2,1)S(1)} async-done(((bf16[32,16,256]{2,1,0:T(8,128)(2,1)}), bf16[32,16,256]{2,1,0:T(8,128)(2,1)S(1)}, u32[]{:S(2)}, u32[]{:S(2)}) %all-to-all-start.4) | async-done | bytes 262176 | tf_op jit(solution)/shard_map/all_to_all | solution.py:215
  247.5 1.2 gather_fusion.1
  249.1 0.6 fusion.11
  (81 shorter events, 6.3 us)
Async XLA Ops:
  6.5 150.8 %copy-start = (bf16[1,128,4096]{2,1,0:T(8,128)(2,1)S(1)}, bf16[1,128,4096]{2,1,0:T(8,128)(2,1)}, u32[]{:S(2)}) copy-start(bf16[1,128,4096]{2,1,0:T(8,128)(2,1)} %param.35) | copy-start | bytes 3145732
  13.0 15.5 %copy-start.9 = (f32[64]{0:T(128)S(1)}, f32[64]{0:T(128)}, u32[]{:S(2)}) copy-start(f32[64]{0:T(128)} %param.26) | copy-start | bytes 772
  13.4 26.3 %copy-start.5 = (f32[4,16,64]{2,1,0:T(8,128)S(1)}, f32[4,16,64]{2,1,0:T(8,128)}, u32[]{:S(2)}) copy-start(f32[4,16,64]{2,1,0:T(8,128)} %param.24) | copy-start | bytes 49156
  13.4 26.7 %copy-start.4 = (bf16[64,128]{1,0:T(8,128)(2,1)S(1)}, bf16[64,128]{1,0:T(8,128)(2,1)}, u32[]{:S(2)}) copy-start(bf16[64,128]{1,0:T(8,128)(2,1)} %param.18) | copy-start | bytes 49156
  13.4 26.7 %copy-start.6 = (f32[4,16,64]{2,1,0:T(8,128)S(1)}, f32[4,16,64]{2,1,0:T(8,128)}, u32[]{:S(2)}) copy-start(f32[4,16,64]{2,1,0:T(8,128)} %param.25) | copy-start | bytes 49156
  13.7 26.8 %copy-start.3 = (bf16[64,4096]{1,0:T(8,128)(2,1)S(1)}, bf16[64,4096]{1,0:T(8,128)(2,1)}, u32[]{:S(2)}) copy-start(bf16[64,4096]{1,0:T(8,128)(2,1)} %param.28) | copy-start | bytes 1572868
  15.6 22.2 %all-to-all-start = ((f32[32,1,1024]{2,1,0:T(1,128)}), f32[32,1,1024]{2,1,0:T(1,128)S(1)}, u32[]{:S(2)}, u32[]{:S(2)}) async-start(f32[32,1,1024]{2,1,0:T(1,128)} %reshape.198), calls=%async_computation | async-start | bytes 262144 | tf_op jit(solution)/shard_map/all_to_all | solution.py:12
  39.3 11.8 %copy-start.7 = (s32[128,2]{0,1:T(2,128)S(1)}, s32[128,2]{0,1:T(2,128)}, u32[]{:S(2)}) copy-start(s32[128,2]{0,1:T(2,128)} %param.31) | copy-start | bytes 3076
  42.0 109.2 %copy-start.2 = (bf16[1,4096,128]{2,1,0:T(8,128)(2,1)S(1)}, bf16[1,4096,128]{2,1,0:T(8,128)(2,1)}, u32[]{:S(2)}) copy-start(bf16[1,4096,128]{2,1,0:T(8,128)(2,1)} %param.33) | copy-start | bytes 3145732
  42.0 35.3 %all-to-all-start.1 = ((bf16[16,128,256]{2,1,0:T(8,128)(2,1)}), bf16[16,128,256]{2,1,0:T(8,128)(2,1)S(1)}, u32[]{:S(2)}, u32[]{:S(2)}) async-start(bf16[16,128,256]{2,1,0:T(8,128)(2,1)} %bitcast.68), calls=%async_computation.1 | async-start | bytes 2097152 | tf_op jit(solution)/shard_map/all_to_all | solution.py:61
  79.1 9.3 %all-to-all-start.2 = ((f32[16,1,128]{2,1,0:T(1,128)}), f32[16,1,128]{2,1,0:T(1,128)S(1)}, u32[]{:S(2)}, u32[]{:S(2)}) async-start(f32[16,1,128]{2,1,0:T(1,128)} %broadcast_in_dim.86), calls=%async_computation.2 | async-start | bytes 16384 | tf_op jit(solution)/shard_map/all_to_all | solution.py:12
  84.4 66.9 %all-gather.2.cloned.1.call-start = ((), (), s32[]{:S(2)}) async-start(), calls=%async_computation.6 | async-start | bytes 4456448 | tf_op jit(solution)/shard_map/all_gather | solution.py:205
  105.9 120.7 %reduce-scatter.2.cloned.1.call-start = ((), (), s32[]{:S(2)}) async-start(), calls=%async_computation.7 | async-start | bytes 4456448 | tf_op jit(solution)/shard_map/reduce_scatter | solution.py:211
  151.2 3.6 %copy-start.1 = (bf16[32,16,4096]{2,1,0:T(8,128)(2,1)S(1)}, bf16[32,16,4096]{2,1,0:T(8,128)(2,1)}, u32[]{:S(2)}) copy-start(bf16[32,16,4096]{2,1,0:T(8,128)(2,1)} %all-gather.2.cloned.1.call-done) | copy-start | bytes 12582916
  157.3 3.5 %copy-start.8 = (f32[128,2]{0,1:T(2,128)S(1)}, f32[128,2]{0,1:T(2,128)}, u32[]{:S(2)}) copy-start(f32[128,2]{0,1:T(2,128)} %param.32) | copy-start | bytes 3076
  226.6 20.9 %all-to-all-start.4 = ((bf16[32,16,256]{2,1,0:T(8,128)(2,1)}), bf16[32,16,256]{2,1,0:T(8,128)(2,1)S(1)}, u32[]{:S(2)}, u32[]{:S(2)}) async-start(bf16[32,16,256]{2,1,0:T(8,128)(2,1)} %bitcast.141), calls=%async_computation.5 | async-start | bytes 524288 | tf_op jit(solution)/shard_map/all_to_all | solution.py:215
Sparse Core Ops, SparseCore 0:
  106.1 45.1 all-gather.1
  160.6 65.9 reduce-scatter.1
where the time goes:
time: 257 us
  waiting for transfers between devices  159 us (62%)
  starting transfers between devices  37 us (14%)
  blocking collectives  15.2 us (6%)
  between operations  13.9 us (5%)
  matrix products  12.5 us (5%)
  local copies, waits for them, and re-layouts  9.55 us (4%)
  other arithmetic  9.4 us (4%)
    reduce_scatter x1, waiting for transfers between devices, per_device(): lax.psum_scatter(down_part.astype(f32).astype(jnp.bfloat16), 'tp', scatte...  65.8 us
    all_gather x1, waiting for transfers between devices, per_device(): piece = lax.all_gather(arrived, 'tp', axis=2, tiled=True)  45.2 us
    all_to_all x1, waiting for transfers between devices, sent_and_summed(): lax.all_to_all(in_blocks(array, dim, length), axis, 0, 0, tiled=True)  24.5 us
    all_to_all x2, starting transfers between devices, copy_for_each(): return lax.all_to_all(copies, axis, split_axis=0, concat_axis=0, tiled=True)  18.1 us
    all_to_all x1, blocking collectives, per_device(): lax.all_to_all(dispatch, 'sp', split_axis=0, concat_axis=0, tiled=True)  15.2 us
    all_to_all x2, waiting for transfers between devices, copy_for_each(): return lax.all_to_all(copies, axis, split_axis=0, concat_axis=0, tiled=True)  12.5 us
    all_to_all x1, waiting for transfers between devices, per_device(): lax.all_to_all(expert_out, 'sp', split_axis=0, concat_axis=0, tiled=True)  11 us
    all_to_all x1, starting transfers between devices, per_device(): lax.all_to_all(expert_out, 'sp', split_axis=0, concat_axis=0, tiled=True)  9.71 us
  transfers between devices with their start and end apart: 6, of which 6 were waited for; matrix products, arithmetic and copies ran while one was open for 1% of the time, Pallas kernels for 0%

commit v1 on v0

--- a/solution.py
+++ b/solution.py
@@ -202,7 +202,9 @@
         experts, capacity, d_local
     )
     arrived = lax.all_to_all(dispatch, "sp", split_axis=0, concat_axis=0, tiled=True)
-    piece = lax.all_gather(arrived, "tp", axis=2, tiled=True)
+    piece = jnp.concatenate(
+        lax.all_to_all(jnp.stack([arrived] * lax.axis_size("tp")), "tp", 0, 0), axis=2
+    )
     gate_part = jnp.einsum("snd,df->snf", piece, gate_w, preferred_element_type=f32)
     up_part = jnp.einsum("snd,df->snf", piece, up_w, preferred_element_type=f32)
     hidden = (jax.nn.silu(gate_part) * up_part).astype(bf16)

time: 257 us -> 304 us (1.18)
  blocking collectives: 15.2 us -> 116 us
  waiting for transfers between devices: 159 us -> 107 us
  matrix products: 12.5 us -> 8.95 us
    all_to_all x0 -> x1, blocking collectives: none -> 101 us  [per_device(): lax.all_to_all(jnp.stack([arrived] * lax.axis_size('tp')), 'tp', 0, 0)]
    all_gather x1 -> x0, waiting for transfers between devices: 45.2 us -> none  [per_device(): piece = lax.all_gather(arrived, 'tp', axis=2, tiled=True)]
    reduce_scatter x1, waiting for transfers between devices: 65.8 us -> 58.8 us  [per_device(): lax.psum_scatter(down_part.astype(f32).astype(jnp.bfloat16), 'tp', scatte...]
  transfers between devices with their start and end apart: 6 -> 5, of which waited for: 6 -> 5; matrix products, arithmetic and copies ran while one was open for 1% -> 1% of each run, Pallas kernels for 0% -> 0%
where the time goes in v1:
time: 304 us; the launch traced here: 303 us
  blocking collectives  116 us (38%)
  waiting for transfers between devices  107 us (35%)
  starting transfers between devices  37 us (12%)
  between operations  13.9 us (5%)
  local copies, waits for them, and re-layouts  11.2 us (4%)
  other arithmetic  9.4 us (3%)
  matrix products  8.95 us (3%)
    all_to_all x1, blocking collectives, per_device(): lax.all_to_all(jnp.stack([arrived] * lax.axis_size('tp')), 'tp', 0, 0)  101 us
    reduce_scatter x1, waiting for transfers between devices, per_device(): lax.psum_scatter(down_part.astype(f32).astype(jnp.bfloat16), 'tp', scatte...  58.8 us
    all_to_all x1, waiting for transfers between devices, sent_and_summed(): lax.all_to_all(in_blocks(array, dim, length), axis, 0, 0, tiled=True)  24.5 us
    all_to_all x2, starting transfers between devices, copy_for_each(): return lax.all_to_all(copies, axis, split_axis=0, concat_axis=0, tiled=True)  18.1 us
    all_to_all x1, blocking collectives, per_device(): lax.all_to_all(dispatch, 'sp', split_axis=0, concat_axis=0, tiled=True)  14.3 us
    all_to_all x2, waiting for transfers between devices, copy_for_each(): return lax.all_to_all(copies, axis, split_axis=0, concat_axis=0, tiled=True)  12.5 us
    all_to_all x1, waiting for transfers between devices, per_device(): lax.all_to_all(expert_out, 'sp', split_axis=0, concat_axis=0, tiled=True)  11 us
    all_to_all x1, starting transfers between devices, per_device(): lax.all_to_all(expert_out, 'sp', split_axis=0, concat_axis=0, tiled=True)  9.89 us
  transfers between devices with their start and end apart: 5, of which 5 were waited for; matrix products, arithmetic and copies ran while one was open for 1% of the time, Pallas kernels for 0%

profile of v1, /device:TPU:25, one launch (start us, length us, event | category | flops | bytes accessed | tf_op | source)
XLA Modules:
  0.0 303.0 jit_solution(1933098109671790382)
XLA Ops:
  6.5 0.7 exp.13
  7.3 0.8 fusion.57
  8.1 1.1 fusion.42
  9.2 1.1 fusion.46
  10.3 0.9 subtract_add_fusion.6
  11.2 1.0 add_add_fusion.5
  14.8 0.8 reshape.208
  15.6 12.9 %all-to-all-start = ((f32[32,1,1024]{2,1,0:T(1,128)}), f32[32,1,1024]{2,1,0:T(1,128)S(1)}, u32[]{:S(2)}, u32[]{:S(2)}) async-start(f32[32,1,1024]{2,1,0:T(1,128)} %reshape.208), calls=%async_computation | async-start | bytes 262144 | tf_op jit(solution)/shard_map/all_to_all | solution.py:12
  28.6 9.2 %all-to-all-done = f32[32,1,1024]{2,1,0:T(1,128)S(1)} async-done(((f32[32,1,1024]{2,1,0:T(1,128)}), f32[32,1,1024]{2,1,0:T(1,128)S(1)}, u32[]{:S(2)}, u32[]{:S(2)}) %all-to-all-start) | async-done | bytes 131104 | tf_op jit(solution)/shard_map/all_to_all | solution.py:12
  38.4 1.0 reduce.12
  41.0 1.1 copy.121
  42.1 9.0 %all-to-all-start.1 = ((bf16[16,128,256]{2,1,0:T(8,128)(2,1)}), bf16[16,128,256]{2,1,0:T(8,128)(2,1)S(1)}, u32[]{:S(2)}, u32[]{:S(2)}) async-start(bf16[16,128,256]{2,1,0:T(8,128)(2,1)} %bitcast.71), calls=%async_computation.1 | async-start | bytes 2097152 | tf_op jit(solution)/shard_map/all_to_all | solution.py:61
  51.5 0.6 reduce-window.6
  52.8 24.5 %all-to-all-done.1 = bf16[16,128,256]{2,1,0:T(8,128)(2,1)S(1)} async-done(((bf16[16,128,256]{2,1,0:T(8,128)(2,1)}), bf16[16,128,256]{2,1,0:T(8,128)(2,1)S(1)}, u32[]{:S(2)}, u32[]{:S(2)}) %all-to-all-start.1) | async-done | bytes 1048608 | tf_op jit(solution)/shard_map/all_to_all | solution.py:61
  77.4 0.9 add_convert_fusion
  78.4 0.6 broadcast_in_dim.86
  79.0 5.2 %all-to-all-start.2 = ((f32[16,1,128]{2,1,0:T(1,128)}), f32[16,1,128]{2,1,0:T(1,128)S(1)}, u32[]{:S(2)}, u32[]{:S(2)}) async-start(f32[16,1,128]{2,1,0:T(1,128)} %broadcast_in_dim.86), calls=%async_computation.2 | async-start | bytes 16384 | tf_op jit(solution)/shard_map/all_to_all | solution.py:12
  84.3 0.8 dynamic_slice.7
  85.1 3.2 %all-to-all-done.2 = f32[16,1,128]{2,1,0:T(1,128)S(1)} async-done(((f32[16,1,128]{2,1,0:T(1,128)}), f32[16,1,128]{2,1,0:T(1,128)S(1)}, u32[]{:S(2)}, u32[]{:S(2)}) %all-to-all-start.2) | async-done | bytes 8224 | tf_op jit(solution)/shard_map/all_to_all | solution.py:12
  88.5 2.0 gather_fusion
  90.6 14.3 %all_to_all.31 = bf16[32,16,256]{2,1,0:T(8,128)(2,1)S(1)} all-to-all(bf16[32,16,256]{2,1,0:T(8,128)(2,1)S(1)} %broadcast_select_fusion), channel_id=1, replica_groups=mesh['sp'=32,'tp'=16] {'sp'}, dimensions={0} | all-to-all | bytes 524288 | tf_op jit(solution)/shard_map/all_to_all | solution.py:204
  105.4 101.4 %all_to_all.32 = bf16[16,32,16,256]{3,2,1,0:T(8,128)(2,1)S(1)} all-to-all(bf16[16,32,16,256]{3,2,1,0:T(8,128)(2,1)S(1)} %stack.2), channel_id=1, replica_groups=mesh['sp'=32,'tp'=16] {'tp'}, dimensions={0} | all-to-all | bytes 8388608 | tf_op jit(solution)/shard_map/all_to_all | solution.py:206
  206.8 0.5 copy.118
  207.4 0.7 copy-done.1
  208.0 1.2 fusion.5
  209.3 1.2 fusion
  210.6 3.2 %convolution_convert_fusion = bf16[512,4096]{1,0:T(8,128)(2,1)} fusion(bf16[512,128]{1,0:T(8,128)(2,1)S(1)} %bitcast.146, bf16[1,128,4096]{2,1,0:T(8,128)(2,1)S(1)} %copy-done), kind=kOutput, calls=%fused_computation.2 | convolution fusion | flops 538968064 | bytes 5373952 | tf_op jit(solution)/shard_map/dot_general | solution.py:212
  214.0 58.8 %reduce-scatter.2.cloned.1.call-done = bf16[512,256]{1,0:T(8,128)(2,1)} async-done(((bf16[512,4096]{1,0:T(8,128)(2,1)}), bf16[512,256]{1,0:T(8,128)(2,1)}) %reduce-scatter.2.cloned.1.call-update) | async-done | bytes 262160 | tf_op jit(solution)/shard_map/reduce_scatter | solution.py:213
  272.8 9.9 %all-to-all-start.5 = ((bf16[32,16,256]{2,1,0:T(8,128)(2,1)}), bf16[32,16,256]{2,1,0:T(8,128)(2,1)S(1)}, u32[]{:S(2)}, u32[]{:S(2)}) async-start(bf16[32,16,256]{2,1,0:T(8,128)(2,1)} %bitcast.147), calls=%async_computation.6 | async-start | bytes 524288 | tf_op jit(solution)/shard_map/all_to_all | solution.py:217
  282.9 11.0 %all-to-all-done.5 = bf16[32,16,256]{2,1,0:T(8,128)(2,1)S(1)} async-done(((bf16[32,16,256]{2,1,0:T(8,128)(2,1)}), bf16[32,16,256]{2,1,0:T(8,128)(2,1)S(1)}, u32[]{:S(2)}, u32[]{:S(2)}) %all-to-all-start.5) | async-done | bytes 262176 | tf_op jit(solution)/shard_map/all_to_all | solution.py:217
  293.9 1.2 gather_fusion.1
  295.5 0.6 fusion.11
  (81 shorter events, 7.6 us)
Async XLA Ops:
  6.5 204.0 %copy-start = (bf16[1,128,4096]{2,1,0:T(8,128)(2,1)S(1)}, bf16[1,128,4096]{2,1,0:T(8,128)(2,1)}, u32[]{:S(2)}) copy-start(bf16[1,128,4096]{2,1,0:T(8,128)(2,1)} %param.35) | copy-start | bytes 3145732
  13.0 15.5 %copy-start.8 = (f32[64]{0:T(128)S(1)}, f32[64]{0:T(128)}, u32[]{:S(2)}) copy-start(f32[64]{0:T(128)} %param.26) | copy-start | bytes 772
  13.4 26.3 %copy-start.4 = (f32[4,16,64]{2,1,0:T(8,128)S(1)}, f32[4,16,64]{2,1,0:T(8,128)}, u32[]{:S(2)}) copy-start(f32[4,16,64]{2,1,0:T(8,128)} %param.24) | copy-start | bytes 49156
  13.4 26.7 %copy-start.3 = (bf16[64,128]{1,0:T(8,128)(2,1)S(1)}, bf16[64,128]{1,0:T(8,128)(2,1)}, u32[]{:S(2)}) copy-start(bf16[64,128]{1,0:T(8,128)(2,1)} %param.18) | copy-start | bytes 49156
  13.4 26.7 %copy-start.5 = (f32[4,16,64]{2,1,0:T(8,128)S(1)}, f32[4,16,64]{2,1,0:T(8,128)}, u32[]{:S(2)}) copy-start(f32[4,16,64]{2,1,0:T(8,128)} %param.25) | copy-start | bytes 49156
  13.7 26.8 %copy-start.2 = (bf16[64,4096]{1,0:T(8,128)(2,1)S(1)}, bf16[64,4096]{1,0:T(8,128)(2,1)}, u32[]{:S(2)}) copy-start(bf16[64,4096]{1,0:T(8,128)(2,1)} %param.28) | copy-start | bytes 1572868
  15.6 22.2 %all-to-all-start = ((f32[32,1,1024]{2,1,0:T(1,128)}), f32[32,1,1024]{2,1,0:T(1,128)S(1)}, u32[]{:S(2)}, u32[]{:S(2)}) async-start(f32[32,1,1024]{2,1,0:T(1,128)} %reshape.208), calls=%async_computation | async-start | bytes 262144 | tf_op jit(solution)/shard_map/all_to_all | solution.py:12
  39.4 11.7 %copy-start.6 = (s32[128,2]{0,1:T(2,128)S(1)}, s32[128,2]{0,1:T(2,128)}, u32[]{:S(2)}) copy-start(s32[128,2]{0,1:T(2,128)} %param.31) | copy-start | bytes 3076
  42.1 35.2 %all-to-all-start.1 = ((bf16[16,128,256]{2,1,0:T(8,128)(2,1)}), bf16[16,128,256]{2,1,0:T(8,128)(2,1)S(1)}, u32[]{:S(2)}, u32[]{:S(2)}) async-start(bf16[16,128,256]{2,1,0:T(8,128)(2,1)} %bitcast.71), calls=%async_computation.1 | async-start | bytes 2097152 | tf_op jit(solution)/shard_map/all_to_all | solution.py:61
  79.0 9.3 %all-to-all-start.2 = ((f32[16,1,128]{2,1,0:T(1,128)}), f32[16,1,128]{2,1,0:T(1,128)S(1)}, u32[]{:S(2)}, u32[]{:S(2)}) async-start(f32[16,1,128]{2,1,0:T(1,128)} %broadcast_in_dim.86), calls=%async_computation.2 | async-start | bytes 16384 | tf_op jit(solution)/shard_map/all_to_all | solution.py:12
  84.2 188.6 %reduce-scatter.2.cloned.1.call-start = ((), (), s32[]{:S(2)}) async-start(), calls=%async_computation.7 | async-start | bytes 4456448 | tf_op jit(solution)/shard_map/reduce_scatter | solution.py:213
  206.8 1.2 copy-start.1
  207.3 1.9 copy-start.9
  210.5 3.5 %copy-start.7 = (f32[128,2]{0,1:T(2,128)S(1)}, f32[128,2]{0,1:T(2,128)}, u32[]{:S(2)}) copy-start(f32[128,2]{0,1:T(2,128)} %param.32) | copy-start | bytes 3076
  272.8 21.1 %all-to-all-start.5 = ((bf16[32,16,256]{2,1,0:T(8,128)(2,1)}), bf16[32,16,256]{2,1,0:T(8,128)(2,1)S(1)}, u32[]{:S(2)}, u32[]{:S(2)}) async-start(bf16[32,16,256]{2,1,0:T(8,128)(2,1)} %bitcast.147), calls=%async_computation.6 | async-start | bytes 524288 | tf_op jit(solution)/shard_map/all_to_all | solution.py:217
Sparse Core Ops, SparseCore 0:
  213.9 58.9 reduce-scatter.1
